TPU v7x, 32 devices: a whole 2x2x4 slice. The times are simulated.
32 devices in a mesh: ep: 4 (over y, x), tp: 8 (over z, core).
Axes of the slice: x: 2, y: 2, z: 4, core: 2. Of those that a mesh axis runs over, the one named last changes fastest.
Arguments:
- queries: bfloat16 [4096, 1024], P('ep', 'tp'), may hold values from -600 to 600
- key_rows: bfloat16 [4096, 128], P('ep'), may hold values from -6 to 6
- value_rows: bfloat16 [4096, 128], P('ep'), may hold values from -48 to 48
- sink_logits: float32 [16], P('tp'), may hold values from 2 to 6
- out_weight: bfloat16 [1024, 2048], P('tp'), may hold values from -0.1875 to 0.1875
- moe_rows: bfloat16 [1024, 2048], P(('ep', 'tp')), may hold values from -6 to 6
- moe_gain: float32 [2048], replicated, may hold values from 0.1 to 1.9
- routes: int32 [1024, 2], P(('ep', 'tp')), may hold values from 0 to 3, all different within a row; in each aligned block of 32 rows (0 to 31, 32 to 63, ...) at most 24 rows name the same one
- route_weight: float32 [1024, 2], P(('ep', 'tp')), may hold values from 0.2 to 1
- gate_weight: bfloat16 [4, 2048, 7168], P('ep', None, 'tp'), may hold values from -0.125 to 0.125
- up_weight: bfloat16 [4, 2048, 7168], P('ep', None, 'tp'), may hold values from -0.125 to 0.125
- down_weight: bfloat16 [4, 7168, 2048], P('ep', 'tp'), may hold values from -0.0625 to 0.0625
Outputs:
- mixer_out: bfloat16 [4096, 2048], P(('ep', 'tp'))
- moe_out: bfloat16 [1024, 2048], P(('ep', 'tp'))
Inputs may be any that keep to these rules, and one draw needn't show every extreme that they name: `routes`: in each aligned block of 32 rows (the rows of one device) no expert is named more than 24 times, a bound that some block reaches; each row names 2 different experts.
All inputs are finite; a program needn't handle non-finite values.
Results may differ from a plain program's by a relative error of at most 0.02.
Values may be sent and summed in bfloat16 or wider, within the bound.
A program may use at most 128 MiB of HBM per device.

v0:
```python
import functools

import jax
import jax.numpy as jnp
from jax import lax
from jax.experimental import pallas as pl
from jax.experimental.pallas import tpu as pltpu
from jax.sharding import PartitionSpec as P

MESH = pl.DeviceIdType.MESH

HEADS = 16
KV_HEADS = 2
HEAD_DIM = 64
WINDOW = 128
TOP = 2


big_negative = -1e30
norm_eps = 1e-05


def passed_along(value, axis, steps):
    count = lax.axis_size(axis)
    initial, last = (max(0, -steps), min(count, count - steps))
    return lax.ppermute(value, axis, [(source, source + steps) for source in range(initial, last)])


def layer_normed(inputs, gain):
    values = inputs.astype(jnp.float32)
    center = values - jnp.mean(values, -1, keepdims=True)
    spread = jnp.mean(center * center, -1, keepdims=True)
    return (center * lax.rsqrt(spread + norm_eps) * gain).astype(jnp.bfloat16)


def attend(queries, key_rows, value_rows, sink_logits):
    total = queries.shape[0]
    heads_here = sink_logits.shape[0]
    blocks = total // WINDOW
    key_head = lax.axis_index("tp") * heads_here // (HEADS // KV_HEADS)
    key_own = lax.dynamic_slice_in_dim(key_rows, key_head * HEAD_DIM, HEAD_DIM, 1)
    value_own = lax.dynamic_slice_in_dim(value_rows, key_head * HEAD_DIM, HEAD_DIM, 1)
    last_rows = jnp.concatenate([key_own[total - WINDOW :], value_own[total - WINDOW :]], 1)
    earlier = passed_along(last_rows, "ep", 1)
    key_ext = jnp.concatenate([earlier[:, :HEAD_DIM], key_own], 0)
    value_ext = jnp.concatenate([earlier[:, HEAD_DIM:], value_own], 0)
    key_blocks = jnp.concatenate(
        [
            key_ext[:total].reshape(blocks, WINDOW, HEAD_DIM),
            key_ext[WINDOW:].reshape(blocks, WINDOW, HEAD_DIM),
        ],
        1,
    )
    value_blocks = jnp.concatenate(
        [
            value_ext[:total].reshape(blocks, WINDOW, HEAD_DIM),
            value_ext[WINDOW:].reshape(blocks, WINDOW, HEAD_DIM),
        ],
        1,
    )
    query_blocks = queries.reshape(blocks, WINDOW, heads_here, HEAD_DIM)
    scores = jnp.einsum(
        "nqhd,nkd->nhqk", query_blocks, key_blocks, preferred_element_type=jnp.float32
    ) * HEAD_DIM ** (-0.5)
    anchor = lax.axis_index("ep") * total
    block_base = anchor + jnp.arange(blocks, dtype=jnp.int32)[:, None, None] * WINDOW
    query_pos = block_base + jnp.arange(WINDOW, dtype=jnp.int32)[None, :, None]
    key_pos = block_base - WINDOW + jnp.arange(2 * WINDOW, dtype=jnp.int32)[None, None, :]
    allowed = ((key_pos <= query_pos) & (key_pos > query_pos - WINDOW) & (key_pos >= 0))[:, None]
    masked = jnp.where(allowed, scores, big_negative)
    sinks = sink_logits[None, :, None]
    row_max = jnp.maximum(jnp.max(masked, -1), sinks)
    powers = jnp.where(allowed, jnp.exp(masked - row_max[..., None]), 0.0)
    totals = jnp.sum(powers, -1) + jnp.exp(sinks - row_max)
    attn_probs = (powers / totals[..., None]).astype(jnp.bfloat16)
    attended = jnp.einsum(
        "nhqk,nkd->nqhd", attn_probs, value_blocks, preferred_element_type=jnp.float32
    )
    return attended.astype(jnp.bfloat16).reshape(total, heads_here * HEAD_DIM)


def mixer(queries, key_rows, value_rows, sink_logits, out_weight):
    attended = attend(queries, key_rows, value_rows, sink_logits)
    return lax.psum_scatter(
        jnp.dot(attended, out_weight, preferred_element_type=jnp.float32).astype(jnp.bfloat16),
        "tp",
        scatter_dimension=0,
        tiled=True,
    )


def experts(moe_rows, moe_gain, routes, route_weight, gate_weight, up_weight, down_weight):
    row_count = moe_rows.shape[0]
    width_all = moe_rows.shape[1]
    expert_count = gate_weight.shape[0] * lax.axis_size("ep")
    capacity = 3 * row_count * TOP // (2 * expert_count)
    normed = layer_normed(moe_rows, moe_gain)
    chosen = routes.reshape(-1)
    onehot = (chosen[:, None] == jnp.arange(expert_count, dtype=jnp.int32)[None, :]).astype(
        jnp.int32
    )
    earlier_count = jnp.cumsum(onehot, 0) - onehot
    slot_index = jnp.sum(earlier_count * onehot, 1)
    target = chosen * capacity + slot_index
    matches = target[None, :] == jnp.arange(expert_count * capacity, dtype=jnp.int32)[:, None]
    dispatch_map = jnp.sum(matches.reshape(expert_count * capacity, row_count, TOP), -1).astype(
        jnp.bfloat16
    )
    buffer = jnp.dot(dispatch_map, normed, preferred_element_type=jnp.float32).astype(jnp.bfloat16)
    buffer = buffer.reshape(expert_count, capacity, width_all)
    gate_mat = gate_weight[0]
    up_mat = up_weight[0]
    down_mat = down_weight[0]
    received = lax.all_to_all(buffer, "ep", split_axis=0, concat_axis=0, tiled=True)
    total = received.shape[0] * received.shape[1]
    flat_rows = received.reshape(total, width_all)
    shard_rows = lax.all_gather(flat_rows, "tp", axis=0, tiled=True)
    gate_val = jnp.dot(shard_rows, gate_mat, preferred_element_type=jnp.float32)
    up_val = jnp.dot(shard_rows, up_mat, preferred_element_type=jnp.float32)
    hidden = (jax.nn.silu(gate_val) * up_val).astype(jnp.bfloat16)
    summed = lax.psum_scatter(
        jnp.dot(hidden, down_mat, preferred_element_type=jnp.float32).astype(jnp.bfloat16),
        "tp",
        scatter_dimension=0,
        tiled=True,
    )
    results = summed.reshape(received.shape)
    returned = lax.all_to_all(results, "ep", split_axis=0, concat_axis=0, tiled=True)
    weights_flat = route_weight.reshape(-1)
    combine_map = jnp.sum(
        jnp.where(matches, weights_flat[None, :], 0.0).reshape(
            expert_count * capacity, row_count, TOP
        ),
        -1,
    )
    returned_flat = returned.reshape(expert_count * capacity, width_all).astype(jnp.float32)
    moe_out = lax.dot_general(
        combine_map, returned_flat, (((0,), (0,)), ((), ())), precision=lax.Precision.HIGHEST
    )
    return moe_out.astype(jnp.bfloat16)


def fused_kernel(
    groups,
    ranks,
    q_ref,
    key_ref,
    value_ref,
    tile_ref,
    rows_ref,
    gain_ref,
    ow_hbm,
    gate_hbm,
    up_hbm,
    down_hbm,
    mix_ref,
    moe_ref,
    x_buf,
    p_buf,
    r1_buf,
    r2_buf,
    r3_buf,
    ru_buf,
    rd_buf,
    w_buf,
    qb_buf,
    tiles,
    halo,
    kdup,
    vdup,
    att,
    gate_w,
    up_w,
    down_w,
    load_sem,
    tile_ss,
    tile_rs,
    q_ss,
    q_rs,
    halo_ss,
    halo_rs,
    up_ss,
    up_rs,
    dn_ss,
    dn_rs,
    pa_ss,
    pa_rs,
    x1_ss,
    x1_rs,
    x2_ss,
    x2_rs,
    wu_ss,
    wu_rs,
    wd_ss,
    wd_rs,
    wp_ss,
    wp_rs,
    wx_ss,
    wx_rs,
    wq_ss,
    wq_rs,
    s1_ss,
    s1_rs,
    s2_ss,
    s2_rs,
    s3_ss,
    s3_rs,
    ru_ss,
    ru_rs,
    rd_ss,
    rd_rs,
):
    chips = ranks // 2
    total = groups * ranks
    e, t = lax.axis_index("ep"), lax.axis_index("tp")
    z, c = lax.div(t, 2), lax.rem(t, 2)
    y, x = lax.div(e, 2), lax.rem(e, 2)
    me = e * ranks + t
    ex, ey, e3 = e + 1 - 2 * x, e + 2 - 4 * y, 3 - e
    e1 = ex * (1 - c) + ey * c
    e2 = ey * (1 - c) + ex * c
    other = t + 1 - 2 * c
    oc = 1 - c
    columns = (e, e1, e2, e3)
    pending = []

    def remote(src, dst, ss, rs, to):
        return pltpu.make_async_remote_copy(
            src_ref=src, dst_ref=dst, send_sem=ss, recv_sem=rs, device_id=to, device_id_type=MESH
        )

    def send(src, dst, ss, rs, to, when=None):
        copy = remote(src, dst, ss, rs, to)
        pending.append((when, copy))
        if when is None:
            copy.start()
        else:
            pl.when(when)(copy.start)

    def received(dst, ss, rs):
        remote(dst, dst, ss, rs, (e, other)).wait_recv()

    loads = [
        pltpu.make_async_copy(ow_hbm, w_buf.at[t], load_sem.at[0]),
        pltpu.make_async_copy(gate_hbm.at[0], gate_w, load_sem.at[1]),
        pltpu.make_async_copy(up_hbm.at[0], up_w, load_sem.at[2]),
        pltpu.make_async_copy(down_hbm.at[0], down_w, load_sem.at[3]),
    ]
    for load in loads:
        load.start()

    barrier = pltpu.get_barrier_semaphore()

    @pl.loop(1, total)
    def _(j):
        to = lax.rem(me + j, total)
        pl.semaphore_signal(
            barrier,
            inc=1,
            device_id=(lax.div(to, ranks), lax.rem(to, ranks)),
            device_id_type=MESH,
        )

    values = rows_ref[...].astype(jnp.float32)
    center = values - jnp.mean(values, -1, keepdims=True)
    spread = jnp.mean(center * center, -1, keepdims=True)
    x_buf[e, z, c] = (center * lax.rsqrt(spread + norm_eps) * gain_ref[...]).astype(jnp.bfloat16)
    tiles[me] = tile_ref[...]
    qb_buf[t] = q_ref[pl.ds(pl.multiple_of(t * WINDOW, WINDOW), WINDOW), :]

    pl.semaphore_wait(barrier, total - 1)

    piece_rows = rows_ref.shape[0] // 2

    def spread_block(zz, up, down, when):
        block = x_buf.at[e, zz, c]
        if up:
            ok = z < chips - 1
            ok = ok if when is None else ok & when
            for h in range(2):
                part = block.at[pl.ds(h * piece_rows, piece_rows), :]
                at = zz * 2 + h
                if when is not None:
                    wait = functools.partial(received, part, up_ss.at[at], up_rs.at[at])
                    pl.when(when)(wait)
                send(part, part, up_ss.at[at], up_rs.at[at], (e, t + 2), ok)
        if down:
            ok = z > 0
            ok = ok if when is None else ok & when
            for h in range(2):
                part = block.at[pl.ds(h * piece_rows, piece_rows), :]
                at = zz * 2 + h
                if when is not None:
                    wait = functools.partial(received, part, dn_ss.at[at], dn_rs.at[at])
                    pl.when(when)(wait)
                send(part, part, dn_ss.at[at], dn_rs.at[at], (e, t - 2), ok)
        send(block, block, x1_ss.at[zz], x1_rs.at[zz], (e1, t), when)
        send(block, block, x2_ss.at[zz], x2_rs.at[zz], (e2, t), when)
        send(block, block, pa_ss.at[zz], pa_rs.at[zz], (e, other), when)

    spread_block(z, True, True, None)

    last = key_ref.shape[0] - WINDOW
    gives = (t == 0) & (e < groups - 1)
    takes = (t == 0) & (e > 0)
    for i, source in enumerate((key_ref, value_ref)):
        send(
            source.at[pl.ds(last, WINDOW), :],
            halo.at[i],
            halo_ss.at[i],
            halo_rs.at[i],
            (lax.rem(e + 1, groups), t),
            gives,
        )

    def from_first(k):
        sides = ((z, None),) if k == 0 else ((z - k, z >= k), (z + k, z + k < chips))
        for zz, when in sides:
            safe = jnp.clip(zz, 0, chips - 1)
            block = x_buf.at[e1, safe, c]
            wait = functools.partial(received, block, x1_ss.at[safe], x1_rs.at[safe])
            wait() if when is None else pl.when(when)(wait)
            slot = chips + safe
            send(block, block, x2_ss.at[slot], x2_rs.at[slot], (e2, t), when)
            send(block, block, pa_ss.at[slot], pa_rs.at[slot], (e, other), when)

    third = w_buf.shape[1] // 4
    side = x * (1 - c) + y * c
    carried = pl.ds(pl.multiple_of(side * third, third), 3 * third)
    given = pl.ds(pl.multiple_of(3 * side * third, third), third)
    taken = pl.ds(pl.multiple_of(3 * (1 - side) * third, third), third)

    other_side = x * c + y * (1 - c)
    other_carried = pl.ds(pl.multiple_of(other_side * third, third), 3 * third)
    other_taken = pl.ds(pl.multiple_of(3 * (1 - other_side) * third, third), third)

    def weight_copies(zz, up, down, when):
        block = w_buf.at[zz * 2 + c, carried, :]
        copies = []
        if up:
            ok = z < chips - 1
            ok = ok if when is None else ok & when
            copies.append((ok, remote(block, block, wu_ss.at[zz], wu_rs.at[zz], (e, t + 2))))
        if down:
            ok = z > 0
            ok = ok if when is None else ok & when
            copies.append((ok, remote(block, block, wd_ss.at[zz], wd_rs.at[zz], (e, t - 2))))
        copies.append((when, remote(block, block, wp_ss.at[zz], wp_rs.at[zz], (e, other))))
        if when is None:
            rest = w_buf.at[zz * 2 + c, taken, :]
            copies.append((when, remote(rest, rest, wq_ss.at[zz], wq_rs.at[zz], (e, other))))
        else:
            piece = w_buf.at[zz * 2 + c, given, :]
            copies.append((when, remote(piece, piece, wx_ss.at[zz], wx_rs.at[zz], (e1, t))))
        return copies

    def spread_weight(zz, up, down, when):
        for ok, copy in weight_copies(zz, up, down, when):
            copy.start() if ok is None else pl.when(ok)(copy.start)

    def pass_weight(k):
        below, has_below = jnp.maximum(z - k, 0), z >= k
        above, has_above = jnp.minimum(z + k, chips - 1), z + k < chips

        @pl.when(has_below)
        def _():
            received(w_buf.at[below * 2 + c, carried, :], wu_ss.at[below], wu_rs.at[below])

        spread_weight(below, True, False, has_below)

        @pl.when(has_above)
        def _():
            received(w_buf.at[above * 2 + c, carried, :], wd_ss.at[above], wd_rs.at[above])

        spread_weight(above, False, True, has_above)

    for k in range(1, chips):
        below, has_below = jnp.maximum(z - k, 0), z >= k
        above, has_above = jnp.minimum(z + k, chips - 1), z + k < chips

        spread_block(below, True, False, has_below)

        spread_block(above, False, True, has_above)
        from_first(k - 1)
    from_first(chips - 1)

    @pl.loop(1, total)
    def _(j):
        to = lax.rem(me + j, total)
        remote(
            tile_ref,
            tiles.at[me],
            tile_ss.at[j],
            tile_rs.at[j],
            (lax.div(to, ranks), lax.rem(to, ranks)),
        ).start()

    @pl.loop(1, ranks)
    def _(j):
        tt = lax.rem(t + j, ranks)
        remote(
            q_ref.at[pl.ds(pl.multiple_of(tt * WINDOW, WINDOW), WINDOW), :],
            qb_buf.at[t],
            q_ss.at[j],
            q_rs.at[j],
            (e, tt),
        ).start()

    loads[0].wait()
    spread_weight(z, True, True, None)


    for load in loads[1:]:
        load.wait()

    row_count = rows_ref.shape[0]
    width = rows_ref.shape[1]
    diagonal = lax.broadcasted_iota(jnp.int32, (row_count, 128), 0) == lax.broadcasted_iota(
        jnp.int32, (row_count, 128), 1
    )

    def column_of(i):
        xi = x + lax.rem(i, 2) * (1 - 2 * x)
        yi = y + lax.div(i, 2) * (1 - 2 * y)
        return yi * 2 + xi

    def partner_column(slot_column, slot):
        for zz in range(chips):
            where = slot * chips + zz
            received(x_buf.at[slot_column, zz, oc], pa_ss.at[where], pa_rs.at[where])

    def from_second(slot):
        column = e2 if slot == 0 else e3
        for zz in range(chips):
            where = slot * chips + zz
            block = x_buf.at[column, zz, c]
            received(block, x2_ss.at[where], x2_rs.at[where])
            to = (2 + slot) * chips + zz
            remote(block, block, pa_ss.at[to], pa_rs.at[to], (e, other)).start()

    far_first = []
    for k in range(chips - 1, 0, -1):
        far_first.append((jnp.maximum(z - k, 0), z >= k))
        far_first.append((jnp.minimum(z + k, chips - 1), z + k < chips))
    far_first.append((z, None))

    def fold(i):
        column = column_of(i)
        received(r1_buf.at[i], s1_ss.at[i], s1_rs.at[i])
        for zz in range(chips):
            p_buf[column, zz, c] = (
                p_buf[column, zz, c].astype(jnp.float32) + r1_buf[i, zz].astype(jnp.float32)
            ).astype(jnp.bfloat16)

        @pl.when((column == e2) | (column == e3))
        def _():
            slot = jnp.where(column == e3, 1, 0)
            for zz, when in far_first:
                place = slot * chips + zz
                copy = remote(
                    p_buf.at[column, zz, c],
                    r2_buf.at[slot, zz],
                    s2_ss.at[place],
                    s2_rs.at[place],
                    (e2, t),
                )
                copy.start() if when is None else pl.when(when)(copy.start)

    @pl.loop(0, groups)
    def _(i):
        column = column_of(i)

        @pl.when(i == 0)
        def _():
            partner_column(e, 0)

        @pl.when(i == 1)
        def _():
            from_second(0)
            partner_column(e1, 2)
            partner_column(e2, 1)

        @pl.when(i == 3)
        def _():
            from_second(1)
            partner_column(e3, 3)

        if chips > 1:

            @pl.when(i == 2)
            def _():
                pass_weight(1)

        rows = x_buf[column].reshape(ranks * row_count, width)
        gate_val = jnp.dot(rows, gate_w[...], preferred_element_type=jnp.float32)
        up_val = jnp.dot(rows, up_w[...], preferred_element_type=jnp.float32)
        hidden = (gate_val / (1.0 + jnp.exp(-gate_val)) * up_val).astype(jnp.bfloat16)

        @pl.when(i > 0)
        def _():
            fold(i - 1)

        @pl.when(i == 0)
        def _():
            @pl.loop(1, total)
            def _(j):
                source = lax.rem(me + total - j, total)
                received(tiles.at[source], tile_ss.at[j], tile_rs.at[j])

        shares = []
        for j in range(ranks):
            line = tiles[column * ranks + j, pl.ds(e, 1), :]
            shares.append(
                jnp.sum(
                    jnp.where(diagonal, jnp.broadcast_to(line, (row_count, 128)), 0.0),
                    -1,
                    keepdims=True,
                )
            )
        share = jnp.concatenate(shares, 0)
        down = jnp.dot(hidden, down_w[...], preferred_element_type=jnp.float32)
        p_buf[column] = (
            (down * share).astype(jnp.bfloat16).reshape(chips, 2, row_count, width)
        )
        remote(
            p_buf.at[column, :, oc], r1_buf.at[i], s1_ss.at[i], s1_rs.at[i], (e, other)
        ).start()

    fold(groups - 1)
    if chips > 2:
        pass_weight(2)

    @pl.loop(1, ranks)
    def _(j):
        source = lax.rem(t + ranks - j, ranks)
        received(qb_buf.at[source], q_ss.at[j], q_rs.at[j])

    lanes = lax.broadcasted_iota(jnp.int32, (WINDOW, 128), 1)
    low = lanes < HEAD_DIM

    def doubled(part, rows, out):
        wide = rows.astype(jnp.float32)
        turned = pltpu.roll(wide, HEAD_DIM, 1)
        place = pl.ds(part * WINDOW, WINDOW)
        out[0, place, :] = jnp.where(low, wide, turned).astype(jnp.bfloat16)
        out[1, place, :] = jnp.where(low, turned, wide).astype(jnp.bfloat16)

    for i, (source, out) in enumerate(((key_ref, kdup), (value_ref, vdup))):
        doubled(1, source[pl.ds(pl.multiple_of(t * WINDOW, WINDOW), WINDOW), :], out)

        @pl.when(t > 0)
        def _():
            before = jnp.maximum(t - 1, 0) * WINDOW
            doubled(0, source[pl.ds(pl.multiple_of(before, WINDOW), WINDOW), :], out)

        @pl.when(takes)
        def _():
            received(halo.at[i], halo_ss.at[i], halo_rs.at[i])
            doubled(0, halo[i], out)

        @pl.when(me == 0)
        def _():
            doubled(0, jnp.zeros((WINDOW, 128), jnp.bfloat16), out)

    query_pos = lax.broadcasted_iota(jnp.int32, (WINDOW, 2 * WINDOW), 0) + WINDOW
    key_pos = lax.broadcasted_iota(jnp.int32, (WINDOW, 2 * WINDOW), 1)
    first = jnp.where(me == 0, WINDOW, 0)
    allowed = (key_pos <= query_pos) & (key_pos > query_pos - WINDOW) & (key_pos >= first)

    def attend_pairs(begin, end):
        @pl.loop(begin, end)
        def _(j):
            pair = qb_buf[j]
            kept = lax.div(j * KV_HEADS, ranks)
            keys, vals = kdup[kept], vdup[kept]
            outs = []
            for i in range(2):
                mine = low if i == 0 else jnp.logical_not(low)
                query = jnp.where(mine, pair, jnp.zeros_like(pair))
                scores = lax.dot_general(
                    query, keys, (((1,), (1,)), ((), ())), preferred_element_type=jnp.float32
                ) * HEAD_DIM ** (-0.5)
                masked = jnp.where(allowed, scores, big_negative)
                sink = tiles[e * ranks + j, groups : groups + 1, i : i + 1]
                row_max = jnp.maximum(jnp.max(masked, -1, keepdims=True), sink)
                powers = jnp.exp(masked - row_max)
                totals = jnp.sum(powers, -1, keepdims=True) + jnp.exp(sink - row_max)
                probs = (powers / totals).astype(jnp.bfloat16)
                outs.append(jnp.dot(probs, vals, preferred_element_type=jnp.float32))
            att[:, pl.ds(pl.multiple_of(j * 128, 128), 128)] = jnp.where(low, outs[0], outs[1]).astype(
                jnp.bfloat16
            )

    half_pairs = ranks // 2
    attend_pairs(0, half_pairs)

    def add_in(block, extra):
        block[...] = (block[...].astype(jnp.float32) + extra[...].astype(jnp.float32)).astype(
            jnp.bfloat16
        )

    for n, (zz, when) in enumerate(far_first):

        def second(zz=zz):
            received(r2_buf.at[1, zz], s2_ss.at[chips + zz], s2_rs.at[chips + zz])
            add_in(p_buf.at[e1, zz, c], r2_buf.at[1, zz])

        second() if when is None else pl.when(when)(second)
        send(p_buf.at[e1, zz, c], r3_buf.at[zz], s3_ss.at[zz], s3_rs.at[zz], (e1, t), when)
        if n % 2:
            step = (n + 1) // 2
            attend_pairs(
                half_pairs + step * half_pairs // (chips + 1),
                half_pairs + (step + 1) * half_pairs // (chips + 1),
            )

    for n, (zz, when) in enumerate(far_first):

        def third_sum(zz=zz):
            received(r2_buf.at[0, zz], s2_ss.at[zz], s2_rs.at[zz])
            received(r3_buf.at[zz], s3_ss.at[zz], s3_rs.at[zz])
            block = p_buf.at[e, zz, c]
            block[...] = (
                block[...].astype(jnp.float32)
                + r2_buf[0, zz].astype(jnp.float32)
                + r3_buf[zz].astype(jnp.float32)
            ).astype(jnp.bfloat16)

        third_sum() if when is None else pl.when(when)(third_sum)
        if when is None:
            continue
        if n % 2:
            inner, buf, ss, rs, to = z > 0, ru_buf, ru_ss, ru_rs, t + 2
        else:
            inner, buf, ss, rs, to = z < chips - 1, rd_buf, rd_ss, rd_rs, t - 2

        for h in range(2):
            rows = pl.ds(h * piece_rows, piece_rows)
            at = zz * 2 + h

            def chain_sum(zz=zz, rows=rows, at=at):
                received(buf.at[zz, rows, :], ss.at[at], rs.at[at])
                add_in(p_buf.at[e, zz, c, rows, :], buf.at[zz, rows, :])

            pl.when(when & inner)(chain_sum)
            send(
                p_buf.at[e, zz, c, rows, :], buf.at[zz, rows, :], ss.at[at], rs.at[at], (e, to), when
            )

    attend_pairs(half_pairs + chips * half_pairs // (chips + 1), ranks)
    for k in range(3, chips):
        pass_weight(k)
    for zz in range(chips):

        @pl.when(z != zz)
        def _():
            received(w_buf.at[zz * 2 + c, taken, :], wx_ss.at[zz], wx_rs.at[zz])

        rest = w_buf.at[zz * 2 + c, taken, :]
        send(rest, rest, wq_ss.at[zz], wq_rs.at[zz], (e, other), z != zz)
    for zz in range(chips):
        received(w_buf.at[zz * 2 + oc, other_carried, :], wp_ss.at[zz], wp_rs.at[zz])
        received(w_buf.at[zz * 2 + oc, other_taken, :], wq_ss.at[zz], wq_rs.at[zz])
    mix_ref[...] = jnp.dot(
        att[...], w_buf[...].reshape(ranks * 128, width), preferred_element_type=jnp.float32
    ).astype(jnp.bfloat16)

    @pl.when(z > 0)
    def _():
        for h in range(2):
            part = ru_buf.at[z, pl.ds(h * piece_rows, piece_rows), :]
            received(part, ru_ss.at[z * 2 + h], ru_rs.at[z * 2 + h])
        add_in(p_buf.at[e, z, c], ru_buf.at[z])

    @pl.when(z < chips - 1)
    def _():
        for h in range(2):
            part = rd_buf.at[z, pl.ds(h * piece_rows, piece_rows), :]
            received(part, rd_ss.at[z * 2 + h], rd_rs.at[z * 2 + h])
        add_in(p_buf.at[e, z, c], rd_buf.at[z])

    moe_ref[...] = p_buf[e, z, c]

    pending.extend(weight_copies(z, True, True, None))
    for k in range(1, chips):
        pending.extend(weight_copies(jnp.maximum(z - k, 0), True, False, z >= k))
        pending.extend(
            weight_copies(jnp.minimum(z + k, chips - 1), False, True, z + k < chips)
        )
    for when, copy in pending:
        copy.wait_send() if when is None else pl.when(when)(copy.wait_send)
    for slot in range(2 * chips, 4 * chips):
        block = x_buf.at[e, z, c]
        remote(block, block, pa_ss.at[slot], pa_rs.at[slot], (e, other)).wait_send()

    @pl.loop(0, groups)
    def _(i):
        remote(
            p_buf.at[e, :, oc], r1_buf.at[i], s1_ss.at[i], s1_rs.at[i], (e, other)
        ).wait_send()

    for place in range(2 * chips):
        remote(
            p_buf.at[e2, 0, c], r2_buf.at[0, 0], s2_ss.at[place], s2_rs.at[place], (e2, t)
        ).wait_send()

    @pl.loop(1, ranks)
    def _(j):
        remote(qb_buf.at[t], qb_buf.at[t], q_ss.at[j], q_rs.at[j], (e, other)).wait_send()

    @pl.loop(1, total)
    def _(j):
        remote(tile_ref, tiles.at[me], tile_ss.at[j], tile_rs.at[j], (e, other)).wait_send()


def fused(
    queries,
    key_rows,
    value_rows,
    sink_logits,
    out_weight,
    moe_rows,
    moe_gain,
    routes,
    route_weight,
    gate_weight,
    up_weight,
    down_weight,
):
    groups, ranks = lax.axis_size("ep"), lax.axis_size("tp")
    chips, total = ranks // 2, groups * ranks
    row_count, width = moe_rows.shape
    units = gate_weight.shape[2]
    chosen, weights = routes.T, route_weight.T
    named = chosen[:, None, :] == jnp.arange(groups, dtype=jnp.int32)[None, :, None]
    shares = jnp.sum(jnp.where(named, weights[:, None, :], 0.0), 0)
    tile_rows = -(-(groups + 1) // 8) * 8
    shares = jnp.pad(shares, ((0, tile_rows - groups), (0, 128 - row_count)))
    sinks = jnp.pad(
        sink_logits[None, :], ((groups, tile_rows - groups - 1), (0, 128 - sink_logits.shape[0]))
    )
    tile = shares + sinks
    bf16, f32 = jnp.bfloat16, jnp.float32
    vmem = pltpu.VMEM
    dma = pltpu.SemaphoreType.DMA
    sems = [(4,)]
    for count in (
        total,
        ranks,
        2,
        2 * chips,
        2 * chips,
        4 * chips,
        chips,
        2 * chips,
        chips,
        chips,
        chips,
        chips,
        chips,
        groups,
        2 * chips,
        chips,
        2 * chips,
        2 * chips,
    ):
        sems += [(count,), (count,)]
    block = (row_count, width)
    in_vmem = pl.BlockSpec(memory_space=pltpu.VMEM)
    in_any = pl.BlockSpec(memory_space=pl.ANY)
    return pl.pallas_call(
        functools.partial(fused_kernel, groups, ranks),
        out_shape=(
            jax.ShapeDtypeStruct((queries.shape[0] // ranks, width), bf16),
            jax.ShapeDtypeStruct(block, bf16),
        ),
        in_specs=[in_vmem] * 6 + [in_any] * 4,
        out_specs=(in_vmem, in_vmem),
        scratch_shapes=[
            vmem((groups, chips, 2) + block, bf16),
            vmem((groups, chips, 2) + block, bf16),
            vmem((groups, chips) + block, bf16),
            vmem((2, chips) + block, bf16),
            vmem((chips,) + block, bf16),
            vmem((chips,) + block, bf16),
            vmem((chips,) + block, bf16),
            vmem((ranks,) + out_weight.shape, bf16),
            vmem((ranks, WINDOW, 128), bf16),
            vmem((total, tile_rows, 128), f32),
            vmem((2, WINDOW, 128), bf16),
            vmem((2, 2 * WINDOW, 128), bf16),
            vmem((2, 2 * WINDOW, 128), bf16),
            vmem((WINDOW, ranks * 128), bf16),
            vmem((width, units), bf16),
            vmem((width, units), bf16),
            vmem((units, width), bf16),
        ]
        + [dma(shape) for shape in sems],
        compiler_params=pltpu.CompilerParams(
            collective_id=0, has_side_effects=True, vmem_limit_bytes=60 * 1024 * 1024
        ),
    )(
        queries,
        key_rows,
        value_rows,
        tile,
        moe_rows,
        moe_gain[None, :],
        out_weight,
        gate_weight,
        up_weight,
        down_weight,
    )


def body(
    queries,
    key_rows,
    value_rows,
    sink_logits,
    out_weight,
    moe_rows,
    moe_gain,
    routes,
    route_weight,
    gate_weight,
    up_weight,
    down_weight,
):
    groups, ranks = lax.axis_size("ep"), lax.axis_size("tp")
    fits = groups == 4 and ranks % 2 == 0 and ranks <= 8
    fits = fits and queries.shape == (ranks * WINDOW, 2 * HEAD_DIM)
    fits = fits and key_rows.shape[1] == 128 and moe_rows.shape[0] % 32 == 0
    if fits:
        return fused(
            queries,
            key_rows,
            value_rows,
            sink_logits,
            out_weight,
            moe_rows,
            moe_gain,
            routes,
            route_weight,
            gate_weight,
            up_weight,
            down_weight,
        )
    mixer_out = mixer(queries, key_rows, value_rows, sink_logits, out_weight)
    moe_out = experts(moe_rows, moe_gain, routes, route_weight, gate_weight, up_weight, down_weight)
    return (mixer_out, moe_out)


def solution(mesh):
    in_specs = (
        P("ep", "tp"),
        P("ep", None),
        P("ep", None),
        P("tp"),
        P("tp", None),
        P(("ep", "tp"), None),
        P(),
        P(("ep", "tp"), None),
        P(("ep", "tp"), None),
        P("ep", None, "tp"),
        P("ep", None, "tp"),
        P("ep", "tp", None),
    )
    out_specs = (P(("ep", "tp"), None), P(("ep", "tp"), None))
    return jax.shard_map(body, mesh=mesh, in_specs=in_specs, out_specs=out_specs, check_vma=False)
```

profile of v0, /device:TPU:0, one launch (start us, length us, event | category | flops | bytes accessed | tf_op | source)
XLA Modules:
  0.0 89.1 jit_solution(17460366181312732818)
XLA Ops:
  0.6 0.7 select_reduce_fusion
  1.3 1.3 %pad_add_fusion.tile_ref = f32[8,128]{1,0:T(8,128)} fusion(f32[1,2]{1,0:T(1,128)} %bitcast.7, f32[4,32]{1,0:T(4,128)S(1)} %select_reduce_fusion), kind=kLoop, calls=%fused_computation | loop fusion | flops 1024 | bytes 4616 | tf_op jit(solution)/shard_map/add | solution.py:742
  2.6 83.0 %shard_map.131 = (bf16[128,2048]{1,0:T(8,128)(2,1)}, bf16[32,2048]{1,0:T(8,128)(2,1)}) custom-call(bf16[1024,128]{1,0:T(8,128)(2,1)} %q_ref.1, bf16[1024,128]{1,0:T(8,128)(2,1)} %key_ref.1, bf16[1024,128]{1,0:T(8,128)(2,1)} %value_ref.1, f32[8,128]{1,0:T(8,128)} %pad_add_fusion.tile_ref, bf16[32,2048]{1,0:T(8,128)(2,1)} %rows_ref.1, f32[1,2048]{1,0:T(1,128)} %bitcast.4, ...), custom_call_target="tpu_custom_call" | custom-call | tf_op jit(solution)/shard_map/pallas_call | solution.py:771
  85.6 1.9 %copy.16 = bf16[128,2048]{1,0:T(8,128)(2,1)} copy(bf16[128,2048]{1,0:T(8,128)(2,1)} %get-tuple-element.4) | data formatting | bytes 1048576
  87.5 1.6 %copy.17 = bf16[32,2048]{1,0:T(8,128)(2,1)} copy(bf16[32,2048]{1,0:T(8,128)(2,1)} %get-tuple-element.5) | data formatting | bytes 262144
where the time goes:
time: 89.3 us; the launch traced here: 89.1 us
  Pallas kernels  83 us (93%)
  local copies, waits for them, and re-layouts  3.45 us (4%)
  other arithmetic  1.96 us (2%)
    pallas_call x1, Pallas kernels, fused(): pl.pallas_call(functools.partial(fused_kernel, groups, ranks), out_shape=...  83 us
    unnamed x2, local copies, waits for them, and re-layouts  3.45 us

commit v1 on v0

v1 whole, which is shorter than its diff:
```python
import functools

import jax
import jax.numpy as jnp
from jax import lax
from jax.experimental import pallas as pl
from jax.experimental.pallas import tpu as pltpu
from jax.sharding import PartitionSpec as P

MESH = pl.DeviceIdType.MESH

HEADS = 16
KV_HEADS = 2
HEAD_DIM = 64
WINDOW = 128
TOP = 2


big_negative = -1e30
norm_eps = 1e-05


def passed_along(value, axis, steps):
    count = lax.axis_size(axis)
    initial, last = (max(0, -steps), min(count, count - steps))
    return lax.ppermute(value, axis, [(source, source + steps) for source in range(initial, last)])


def layer_normed(inputs, gain):
    values = inputs.astype(jnp.float32)
    center = values - jnp.mean(values, -1, keepdims=True)
    spread = jnp.mean(center * center, -1, keepdims=True)
    return (center * lax.rsqrt(spread + norm_eps) * gain).astype(jnp.bfloat16)


def attend(queries, key_rows, value_rows, sink_logits):
    total = queries.shape[0]
    heads_here = sink_logits.shape[0]
    blocks = total // WINDOW
    key_head = lax.axis_index("tp") * heads_here // (HEADS // KV_HEADS)
    key_own = lax.dynamic_slice_in_dim(key_rows, key_head * HEAD_DIM, HEAD_DIM, 1)
    value_own = lax.dynamic_slice_in_dim(value_rows, key_head * HEAD_DIM, HEAD_DIM, 1)
    last_rows = jnp.concatenate([key_own[total - WINDOW :], value_own[total - WINDOW :]], 1)
    earlier = passed_along(last_rows, "ep", 1)
    key_ext = jnp.concatenate([earlier[:, :HEAD_DIM], key_own], 0)
    value_ext = jnp.concatenate([earlier[:, HEAD_DIM:], value_own], 0)
    key_blocks = jnp.concatenate(
        [
            key_ext[:total].reshape(blocks, WINDOW, HEAD_DIM),
            key_ext[WINDOW:].reshape(blocks, WINDOW, HEAD_DIM),
        ],
        1,
    )
    value_blocks = jnp.concatenate(
        [
            value_ext[:total].reshape(blocks, WINDOW, HEAD_DIM),
            value_ext[WINDOW:].reshape(blocks, WINDOW, HEAD_DIM),
        ],
        1,
    )
    query_blocks = queries.reshape(blocks, WINDOW, heads_here, HEAD_DIM)
    scores = jnp.einsum(
        "nqhd,nkd->nhqk", query_blocks, key_blocks, preferred_element_type=jnp.float32
    ) * HEAD_DIM ** (-0.5)
    anchor = lax.axis_index("ep") * total
    block_base = anchor + jnp.arange(blocks, dtype=jnp.int32)[:, None, None] * WINDOW
    query_pos = block_base + jnp.arange(WINDOW, dtype=jnp.int32)[None, :, None]
    key_pos = block_base - WINDOW + jnp.arange(2 * WINDOW, dtype=jnp.int32)[None, None, :]
    allowed = ((key_pos <= query_pos) & (key_pos > query_pos - WINDOW) & (key_pos >= 0))[:, None]
    masked = jnp.where(allowed, scores, big_negative)
    sinks = sink_logits[None, :, None]
    row_max = jnp.maximum(jnp.max(masked, -1), sinks)
    powers = jnp.where(allowed, jnp.exp(masked - row_max[..., None]), 0.0)
    totals = jnp.sum(powers, -1) + jnp.exp(sinks - row_max)
    attn_probs = (powers / totals[..., None]).astype(jnp.bfloat16)
    attended = jnp.einsum(
        "nhqk,nkd->nqhd", attn_probs, value_blocks, preferred_element_type=jnp.float32
    )
    return attended.astype(jnp.bfloat16).reshape(total, heads_here * HEAD_DIM)


def mixer(queries, key_rows, value_rows, sink_logits, out_weight):
    attended = attend(queries, key_rows, value_rows, sink_logits)
    return lax.psum_scatter(
        jnp.dot(attended, out_weight, preferred_element_type=jnp.float32).astype(jnp.bfloat16),
        "tp",
        scatter_dimension=0,
        tiled=True,
    )


def experts(moe_rows, moe_gain, routes, route_weight, gate_weight, up_weight, down_weight):
    row_count = moe_rows.shape[0]
    width_all = moe_rows.shape[1]
    expert_count = gate_weight.shape[0] * lax.axis_size("ep")
    capacity = 3 * row_count * TOP // (2 * expert_count)
    normed = layer_normed(moe_rows, moe_gain)
    chosen = routes.reshape(-1)
    onehot = (chosen[:, None] == jnp.arange(expert_count, dtype=jnp.int32)[None, :]).astype(
        jnp.int32
    )
    earlier_count = jnp.cumsum(onehot, 0) - onehot
    slot_index = jnp.sum(earlier_count * onehot, 1)
    target = chosen * capacity + slot_index
    matches = target[None, :] == jnp.arange(expert_count * capacity, dtype=jnp.int32)[:, None]
    dispatch_map = jnp.sum(matches.reshape(expert_count * capacity, row_count, TOP), -1).astype(
        jnp.bfloat16
    )
    buffer = jnp.dot(dispatch_map, normed, preferred_element_type=jnp.float32).astype(jnp.bfloat16)
    buffer = buffer.reshape(expert_count, capacity, width_all)
    gate_mat = gate_weight[0]
    up_mat = up_weight[0]
    down_mat = down_weight[0]
    received = lax.all_to_all(buffer, "ep", split_axis=0, concat_axis=0, tiled=True)
    total = received.shape[0] * received.shape[1]
    flat_rows = received.reshape(total, width_all)
    shard_rows = lax.all_gather(flat_rows, "tp", axis=0, tiled=True)
    gate_val = jnp.dot(shard_rows, gate_mat, preferred_element_type=jnp.float32)
    up_val = jnp.dot(shard_rows, up_mat, preferred_element_type=jnp.float32)
    hidden = (jax.nn.silu(gate_val) * up_val).astype(jnp.bfloat16)
    summed = lax.psum_scatter(
        jnp.dot(hidden, down_mat, preferred_element_type=jnp.float32).astype(jnp.bfloat16),
        "tp",
        scatter_dimension=0,
        tiled=True,
    )
    results = summed.reshape(received.shape)
    returned = lax.all_to_all(results, "ep", split_axis=0, concat_axis=0, tiled=True)
    weights_flat = route_weight.reshape(-1)
    combine_map = jnp.sum(
        jnp.where(matches, weights_flat[None, :], 0.0).reshape(
            expert_count * capacity, row_count, TOP
        ),
        -1,
    )
    returned_flat = returned.reshape(expert_count * capacity, width_all).astype(jnp.float32)
    moe_out = lax.dot_general(
        combine_map, returned_flat, (((0,), (0,)), ((), ())), precision=lax.Precision.HIGHEST
    )
    return moe_out.astype(jnp.bfloat16)


def fused_kernel(
    groups,
    ranks,
    chosen_ref,
    weights_ref,
    sink_ref,
    rows_ref,
    gain_ref,
    q_hbm,
    key_hbm,
    value_hbm,
    ow_hbm,
    gate_hbm,
    up_hbm,
    down_hbm,
    mix_hbm,
    moe_hbm,
    x_buf,
    p_buf,
    r1_buf,
    r2_buf,
    r3_buf,
    rc_buf,
    w_buf,
    qb_buf,
    l_buf,
    halo,
    kdup,
    vdup,
    att,
    hid,
    mix_v,
    q_ref,
    key_ref,
    value_ref,
    gate_w,
    up_w,
    down_w,
    load_sem,
    out_sem,
    sem,
    z_rs,
    x1_rs,
    x2_rs,
    pa_rs,
    zl_rs,
    l1_rs,
    l2_rs,
    lp_rs,
    w_rs,
    wp_rs,
    wx_rs,
    wq_rs,
    s1_rs,
    s2_rs,
    s3_rs,
    rc_rs,
    q_rs,
    halo_rs,
):
    chips = ranks // 2
    e, t = lax.axis_index("ep"), lax.axis_index("tp")
    z, c = lax.div(t, 2), lax.rem(t, 2)
    y, x = lax.div(e, 2), lax.rem(e, 2)
    me = e * ranks + t
    ex, ey, e3 = e + 1 - 2 * x, e + 2 - 4 * y, 3 - e
    e1 = ex * (1 - c) + ey * c
    e2 = ey * (1 - c) + ex * c
    other = t + 1 - 2 * c
    oc = 1 - c
    mid = (z > 0) & (z < chips - 1)
    edge = jnp.logical_not(mid)
    row_count, width = rows_ref.shape
    half_rows = row_count // 2
    units = gate_w.shape[1]
    upper = lax.div(z, 2)
    order = (z, z + 1 - 2 * lax.rem(z, 2), 2 - upper, 3 * (1 - upper))

    def plane(i):
        if isinstance(i, int):
            return order[i]
        later = jnp.where(i == 2, order[2], order[3])
        return jnp.where(i == 0, order[0], jnp.where(i == 1, order[1], later))

    def from_above(zz):
        return jnp.where(zz > z, 1, 0)

    def remote(src, dst, ss, rs, to):
        return pltpu.make_async_remote_copy(
            src_ref=src, dst_ref=dst, send_sem=ss, recv_sem=rs, device_id=to, device_id_type=MESH
        )

    ss = [sem.at[k] for k in range(sem.shape[0])]
    (zo_ss, zf_ss, x1_ss, x2_ss, pa_ss, zlo_ss, zlf_ss, l1_ss, l2_ss, lp_ss) = ss[:10]
    (wo_ss, wf_ss, wp_ss, wx_ss, wq_ss, s1_ss, s2_ss, s3_ss, rc_ss, q_ss, halo_ss) = ss[10:]

    def received(dst, rs):
        remote(dst, dst, x1_ss, rs, (e, other)).wait_recv()

    def sent(src, send_sem):
        remote(src, src, send_sem, x1_rs.at[0], (e, other)).wait_send()

    loads = [
        pltpu.make_async_copy(ow_hbm, w_buf.at[t], load_sem.at[0]),
        pltpu.make_async_copy(key_hbm, key_ref, load_sem.at[1]),
        pltpu.make_async_copy(value_hbm, value_ref, load_sem.at[2]),
        pltpu.make_async_copy(q_hbm, q_ref, load_sem.at[3]),
        pltpu.make_async_copy(gate_hbm.at[0], gate_w, load_sem.at[4]),
        pltpu.make_async_copy(up_hbm.at[0], up_w, load_sem.at[5]),
        pltpu.make_async_copy(down_hbm.at[0], down_w, load_sem.at[6]),
    ]
    for load in loads:
        load.start()

    barrier = pltpu.get_barrier_semaphore()

    def greet(to):
        pl.semaphore_signal(barrier, inc=1, device_id=to, device_id_type=MESH)

    for to in ((e, other), (e1, t), (e2, t)):
        greet(to)

    @pl.when(z > 0)
    def _():
        greet((e, t - 2))

    @pl.when(z < chips - 1)
    def _():
        greet((e, t + 2))

    values = rows_ref[...].astype(jnp.float32)
    center = values - jnp.mean(values, -1, keepdims=True)
    spread_of = jnp.mean(center * center, -1, keepdims=True)
    x_buf[z, e, c] = (center * lax.rsqrt(spread_of + norm_eps) * gain_ref[...]).astype(jnp.bfloat16)
    lane = lax.broadcasted_iota(jnp.int32, (1, 128), 1)
    sinks = jnp.zeros((1, 128), jnp.float32)
    for i in range(2):
        sinks = jnp.where(lane == row_count + i, sink_ref[:, i : i + 1], sinks)
    chosen, weights = chosen_ref[...], weights_ref[...]
    for k in range(groups):
        named = jnp.where(chosen == k, weights, 0.0)
        l_buf[z, e, c, k] = sinks
        l_buf[z, e, c, k, :, 0:row_count] = jnp.sum(named, 0, keepdims=True)

    with jax.named_scope("barrier"):
        pl.semaphore_wait(barrier, jnp.where(mid, 5, 4))

    def half(block, h):
        return block.at[pl.ds(h * half_rows, half_rows), :]

    def pair_send(zz, column, x_sems, l_sems, to):
        for buf, (send_sem, recv_sem) in ((x_buf, x_sems), (l_buf, l_sems)):
            piece = buf.at[zz, column, c]
            remote(piece, piece, send_sem, recv_sem, to).start()

    def z_send(zz, to, h, send_sem, line_sem):
        part = half(x_buf.at[zz, e, c], h)
        remote(part, part, send_sem, z_rs.at[zz * 2 + h], to).start()
        if h == 1:
            line = l_buf.at[zz, e, c]
            remote(line, line, line_sem, zl_rs.at[zz], to).start()

    def spread(zz):
        pair_send(zz, e, (x1_ss, x1_rs.at[zz]), (l1_ss, l1_rs.at[zz]), (e1, t))
        pair_send(zz, e, (x2_ss, x2_rs.at[zz]), (l2_ss, l2_rs.at[zz]), (e2, t))
        pair_send(zz, e, (pa_ss, pa_rs.at[zz]), (lp_ss, lp_rs.at[zz]), (e, other))

    @jax.named_scope("arrive")
    def arrive(i):
        zz = plane(i)
        to = (e, t + 2 - 4 * from_above(zz))
        for h in range(2):
            received(half(x_buf.at[zz, e, c], h), z_rs.at[zz * 2 + h])
            if h == 1:
                received(l_buf.at[zz, e, c], zl_rs.at[zz])

            @pl.when(mid)
            def _():
                z_send(zz, to, h, zf_ss, zlf_ss)

        spread(zz)

    @jax.named_scope("from_first")
    def from_first(zz):
        received(x_buf.at[zz, e1, c], x1_rs.at[zz])
        received(l_buf.at[zz, e1, c], l1_rs.at[zz])
        slot = chips + zz
        pair_send(zz, e1, (x2_ss, x2_rs.at[slot]), (l2_ss, l2_rs.at[slot]), (e2, t))
        pair_send(zz, e1, (pa_ss, pa_rs.at[zz]), (lp_ss, lp_rs.at[zz]), (e, other))

    @jax.named_scope("from_second")
    def from_second(zz):
        for slot, column in ((0, e2), (1, e3)):
            where = slot * chips + zz
            received(x_buf.at[zz, column, c], x2_rs.at[where])
            received(l_buf.at[zz, column, c], l2_rs.at[where])
            pair_send(zz, column, (pa_ss, pa_rs.at[zz]), (lp_ss, lp_rs.at[zz]), (e, other))

    @jax.named_scope("from_partner")
    def from_partner(zz):
        received(x_buf.at[zz, :, oc], pa_rs.at[zz])
        received(l_buf.at[zz, :, oc], lp_rs.at[zz])

    third = w_buf.shape[1] // 4
    side = x * (1 - c) + y * c
    carried = pl.ds(pl.multiple_of(side * third, third), 3 * third)
    given = pl.ds(pl.multiple_of(3 * side * third, third), third)
    taken = pl.ds(pl.multiple_of(3 * (1 - side) * third, third), third)
    other_side = x * c + y * (1 - c)
    other_carried = pl.ds(pl.multiple_of(other_side * third, third), 3 * third)
    other_taken = pl.ds(pl.multiple_of(3 * (1 - other_side) * third, third), third)

    def w_send(zz, to, send_sem):
        block = w_buf.at[zz * 2 + c, carried, :]
        remote(block, block, send_sem, w_rs.at[zz], to).start()

    def w_partner(zz):
        block = w_buf.at[zz * 2 + c, carried, :]
        remote(block, block, wp_ss, wp_rs.at[0], (e, other)).start()

    def w_rest(zz):
        rest = w_buf.at[zz * 2 + c, taken, :]
        remote(rest, rest, wq_ss, wq_rs.at[0], (e, other)).start()

    @jax.named_scope("w_arrive")
    def w_arrive(i):
        zz = plane(i)
        received(w_buf.at[zz * 2 + c, carried, :], w_rs.at[zz])

        @pl.when(mid)
        def _():
            w_send(zz, (e, t + 2 - 4 * from_above(zz)), wf_ss)

        piece = w_buf.at[zz * 2 + c, given, :]
        remote(piece, piece, wx_ss, wx_rs.at[zz], (e1, t)).start()
        w_partner(zz)

    def q_send(zz):
        for core in range(2):
            tt = zz * 2 + core

            @pl.when(tt != t)
            def _():
                remote(
                    q_ref.at[pl.ds(pl.multiple_of(tt * WINDOW, WINDOW), WINDOW), :],
                    qb_buf.at[t],
                    q_ss,
                    q_rs.at[z],
                    (e, tt),
                ).start()

    for h in range(2):

        @pl.when(z < chips - 1)
        def _():
            z_send(z, (e, t + 2), h, zo_ss, zlo_ss)

        @pl.when(z > 0)
        def _():
            z_send(z, (e, t - 2), h, zo_ss, zlo_ss)

    spread(z)
    loads[0].wait()
    ahead = (e, t + 2 - 4 * from_above(plane(1)))

    @pl.when(edge)
    def _():
        w_send(z, (e, jnp.where(z == 0, t + 2, t - 2)), wo_ss)

    w_partner(z)
    w_rest(z)
    from_first(z)
    arrive(1)

    @pl.when(mid)
    def _():
        w_send(z, ahead, wo_ss)
        arrive(2)
        arrive(3)
        w_send(z, (e, t - 2 + 4 * from_above(plane(1))), wo_ss)

    from_second(z)
    from_partner(z)
    for load in loads[1:4]:
        load.wait()

    last = key_ref.shape[0] - WINDOW
    gives = (t == 0) & (e < groups - 1)
    takes = (t == 0) & (e > 0)
    for i, source in enumerate((key_ref, value_ref)):
        copy = remote(
            source.at[pl.ds(last, WINDOW), :],
            halo.at[i],
            halo_ss,
            halo_rs.at[0],
            (lax.rem(e + 1, groups), t),
        )
        pl.when(gives)(copy.start)

    q_send(z)
    for load in loads[4:6]:
        load.wait()

    diagonal = lax.broadcasted_iota(jnp.int32, (row_count, 128), 0) == lax.broadcasted_iota(
        jnp.int32, (row_count, 128), 1
    )
    cut = (-(-units // 256) + 1) // 2 * 256
    rows_in_plane = groups * 2 * row_count

    @jax.named_scope("gate_up")
    def gate_up(zz, begin, end):
        rows = x_buf[zz].reshape(rows_in_plane, width)
        gate_val = jnp.dot(rows, gate_w[:, begin:end], preferred_element_type=jnp.float32)
        up_val = jnp.dot(rows, up_w[:, begin:end], preferred_element_type=jnp.float32)
        hid[:, begin:end] = (gate_val / (1.0 + jnp.exp(-gate_val)) * up_val).astype(jnp.bfloat16)

    def add_in(block, extra):
        block[...] = (block[...].astype(jnp.float32) + extra[...].astype(jnp.float32)).astype(
            jnp.bfloat16
        )

    @jax.named_scope("fold")
    def fold(i):
        zz = plane(i)
        received(r1_buf.at[zz], s1_rs.at[zz])
        for n, column in enumerate((e3, e2, e1, e)):
            block = p_buf.at[zz, column, c]
            add_in(block, r1_buf.at[zz, column])
            if n < 2:
                place = (1 - n) * chips + zz
                remote(block, r2_buf.at[1 - n, zz], s2_ss, s2_rs.at[place], (e2, t)).start()

    @jax.named_scope("second")
    def second(i):
        zz = plane(i)
        received(r2_buf.at[1, zz], s2_rs.at[chips + zz])
        block = p_buf.at[zz, e1, c]
        add_in(block, r2_buf.at[1, zz])
        remote(block, r3_buf.at[zz], s3_ss, s3_rs.at[zz], (e1, t)).start()

    @jax.named_scope("third_sum")
    def third_sum(i):
        zz = plane(i)
        received(r2_buf.at[0, zz], s2_rs.at[zz])
        received(r3_buf.at[zz], s3_rs.at[zz])
        block = p_buf.at[zz, e, c]
        block[...] = (
            block[...].astype(jnp.float32)
            + r2_buf[0, zz].astype(jnp.float32)
            + r3_buf[zz].astype(jnp.float32)
        ).astype(jnp.bfloat16)

    @jax.named_scope("chain")
    def chain(i, passing):
        zz = plane(i)
        hops = 2 if passing and i == 3 else 1
        to = (e, t + hops * (4 * from_above(zz) - 2))
        slot = 2 if i == 1 else 3 if passing else i - 2
        for h in range(2):
            part = half(p_buf.at[zz, e, c], h)
            if passing:
                extra = half(rc_buf.at[i - 2], h)
                received(extra, rc_rs.at[(i - 2) * 2 + h])
                add_in(part, extra)
            remote(part, half(rc_buf.at[slot], h), rc_ss, rc_rs.at[slot * 2 + h], to).start()

    @pl.loop(0, groups)
    def _(i):
        zz = plane(i)

        @pl.when(i > 0)
        def _():
            from_second(zz)
            from_partner(zz)
            q_send(zz)

        gate_up(zz, 0, cut)

        @pl.when(i == 0)
        def _():
            from_first(plane(1))
            pl.when(edge)(functools.partial(arrive, 2))

        @pl.when(i == 1)
        def _():
            from_first(plane(2))

        @pl.when(i == 2)
        def _():
            fold(0)

        @pl.when(i == 3)
        def _():
            fold(2)
            second(0)

        gate_up(zz, cut, units)

        @pl.when(i == 0)
        def _():
            loads[6].wait()

        @pl.when(i == 1)
        def _():
            from_first(plane(3))

        @pl.when(i == 2)
        def _():
            fold(1)

        @pl.when(i == 3)
        def _():
            second(1)

        shares = []
        for column in range(groups):
            for core in range(2):
                line = l_buf[zz, column, core, e]
                shares.append(
                    jnp.sum(
                        jnp.where(diagonal, jnp.broadcast_to(line, (row_count, 128)), 0.0),
                        -1,
                        keepdims=True,
                    )
                )
        share = jnp.concatenate(shares, 0)
        with jax.named_scope("down"):
            down = jnp.dot(hid[...], down_w[...], preferred_element_type=jnp.float32)
            p_buf[zz] = (down * share).astype(jnp.bfloat16).reshape(groups, 2, row_count, width)
        remote(p_buf.at[zz, :, oc], r1_buf.at[zz], s1_ss, s1_rs.at[zz], (e, other)).start()

        @pl.when((i == 0) & edge)
        def _():
            arrive(3)

        @pl.when((i == 1) & mid)
        def _():
            w_arrive(1)

        @pl.when((i == 2) & mid)
        def _():
            w_arrive(2)

    third_sum(0)
    third_sum(1)
    chain(1, False)
    second(2)
    fold(3)

    @pl.when(edge)
    def _():
        w_arrive(1)

    @pl.when(mid)
    def _():
        w_arrive(3)

    qb_buf[t] = q_ref[pl.ds(pl.multiple_of(t * WINDOW, WINDOW), WINDOW), :]

    lanes = lax.broadcasted_iota(jnp.int32, (WINDOW, 128), 1)
    low = lanes < HEAD_DIM

    def doubled(part, rows, out):
        wide = rows.astype(jnp.float32)
        turned = pltpu.roll(wide, HEAD_DIM, 1)
        place = pl.ds(part * WINDOW, WINDOW)
        out[0, place, :] = jnp.where(low, wide, turned).astype(jnp.bfloat16)
        out[1, place, :] = jnp.where(low, turned, wide).astype(jnp.bfloat16)

    for i, (source, out) in enumerate(((key_ref, kdup), (value_ref, vdup))):
        doubled(1, source[pl.ds(pl.multiple_of(t * WINDOW, WINDOW), WINDOW), :], out)

        @pl.when(t > 0)
        def _():
            before = jnp.maximum(t - 1, 0) * WINDOW
            doubled(0, source[pl.ds(pl.multiple_of(before, WINDOW), WINDOW), :], out)

        @pl.when(takes)
        def _():
            if i == 0:
                received(halo, halo_rs.at[0])
            doubled(0, halo[i], out)

        @pl.when(me == 0)
        def _():
            doubled(0, jnp.zeros((WINDOW, 128), jnp.bfloat16), out)

    query_pos = lax.broadcasted_iota(jnp.int32, (WINDOW, 2 * WINDOW), 0) + WINDOW
    key_pos = lax.broadcasted_iota(jnp.int32, (WINDOW, 2 * WINDOW), 1)
    first = jnp.where(me == 0, WINDOW, 0)
    allowed = (key_pos <= query_pos) & (key_pos > query_pos - WINDOW) & (key_pos >= first)

    @jax.named_scope("attend")
    def attend_plane(i):
        zz = plane(i)
        if i == 0:
            received(qb_buf.at[0], q_rs.at[zz])
        else:
            received(qb_buf.at[0:2], q_rs.at[zz])

        @pl.loop(0, 2)
        def _(core):
            j = zz * 2 + core
            pair = qb_buf[j]
            kept = lax.div(j * KV_HEADS, ranks)
            keys, vals = kdup[kept], vdup[kept]
            line = l_buf[zz, e, core, e]
            outs = []
            for i in range(2):
                mine_half = low if i == 0 else jnp.logical_not(low)
                query = jnp.where(mine_half, pair, jnp.zeros_like(pair))
                scores = lax.dot_general(
                    query, keys, (((1,), (1,)), ((), ())), preferred_element_type=jnp.float32
                ) * HEAD_DIM ** (-0.5)
                masked = jnp.where(allowed, scores, big_negative)
                sink = line[:, row_count + i : row_count + i + 1]
                row_max = jnp.maximum(jnp.max(masked, -1, keepdims=True), sink)
                powers = jnp.exp(masked - row_max)
                totals = jnp.sum(powers, -1, keepdims=True) + jnp.exp(sink - row_max)
                probs = (powers / totals).astype(jnp.bfloat16)
                outs.append(jnp.dot(probs, vals, preferred_element_type=jnp.float32))
            att[:, pl.ds(pl.multiple_of(j * 128, 128), 128)] = jnp.where(low, outs[0], outs[1]).astype(
                jnp.bfloat16
            )

    attend_plane(0)
    third_sum(2)

    @pl.when(edge)
    def _():
        chain(2, False)

    second(3)
    attend_plane(1)

    @pl.when(mid)
    def _():
        chain(2, True)

    third_sum(3)

    @pl.when(edge)
    def _():
        chain(3, False)
        w_arrive(2)

    attend_plane(2)

    @pl.when(mid)
    def _():
        chain(3, True)

    attend_plane(3)

    @pl.when(edge)
    def _():
        w_arrive(3)

    with jax.named_scope("wwait"):
        for i in range(1, chips):
            zz = plane(i)
            received(w_buf.at[zz * 2 + c, taken, :], wx_rs.at[zz])
            w_rest(zz)
        received(w_buf.at[0:chips, other_carried, :], wp_rs.at[0])
        received(w_buf.at[0:chips, other_taken, :], wq_rs.at[0])
    with jax.named_scope("mix"):
        mix_v[...] = jnp.dot(
            att[...], w_buf[...].reshape(ranks * 128, width), preferred_element_type=jnp.float32
        ).astype(jnp.bfloat16)
    mix_out = pltpu.make_async_copy(mix_v, mix_hbm, out_sem.at[0])
    mix_out.start()

    for slot in (2, 3):
        for h in range(2):
            part = half(rc_buf.at[slot], h)
            with jax.named_scope("last"):
                received(part, rc_rs.at[slot * 2 + h])
                add_in(half(p_buf.at[z, e, c], h), part)

    moe_out = pltpu.make_async_copy(p_buf.at[z, e, c], moe_hbm, out_sem.at[1])
    moe_out.start()

    sent(r1_buf.at[0], x1_ss)
    sent(r1_buf.at[0:2], x2_ss)
    sent(r1_buf, pa_ss)
    sent(l_buf.at[0, :, 0], l1_ss)
    sent(l_buf.at[0], l2_ss)
    sent(l_buf.at[0:2], lp_ss)
    heavy, light = pl.ds(0, 3 * third), pl.ds(0, third)

    @pl.when(edge)
    def _():
        sent(x_buf.at[0, 0, 0], zo_ss)
        sent(l_buf.at[0, 0, 0], zlo_ss)
        sent(w_buf.at[0, heavy, :], wo_ss)

    @pl.when(mid)
    def _():
        sent(x_buf.at[0, 0], zo_ss)
        sent(l_buf.at[0, 0], zlo_ss)
        sent(w_buf.at[0:2, heavy, :], wo_ss)
        sent(r1_buf.at[0, 0:3], zf_ss)
        sent(l_buf.at[0, 0:3, 0], zlf_ss)
        sent(w_buf.at[0:3, heavy, :], wf_ss)

    sent(w_buf.at[0:chips, heavy, :], wp_ss)
    sent(w_buf.at[0:chips, light, :], wq_ss)
    sent(w_buf.at[0 : chips - 1, light, :], wx_ss)
    sent(r1_buf, s1_ss)
    sent(r1_buf.at[0:2], s2_ss)
    sent(r1_buf.at[0], s3_ss)
    sent(r1_buf.at[0, 0:3], rc_ss)
    sent(qb_buf.at[0 : ranks - 1], q_ss)

    @pl.when(gives)
    def _():
        sent(halo, halo_ss)

    with jax.named_scope("outs"):
        mix_out.wait()
        moe_out.wait()


def fused(
    queries,
    key_rows,
    value_rows,
    sink_logits,
    out_weight,
    moe_rows,
    moe_gain,
    routes,
    route_weight,
    gate_weight,
    up_weight,
    down_weight,
):
    groups, ranks = lax.axis_size("ep"), lax.axis_size("tp")
    chips = ranks // 2
    row_count, width = moe_rows.shape
    units = gate_weight.shape[2]
    bf16, f32 = jnp.bfloat16, jnp.float32
    vmem = pltpu.VMEM
    dma = pltpu.SemaphoreType.DMA
    one, two = chips, 2 * chips
    counts = (7, 2, 21, two, one, two, one, one, one, two, one)
    counts += (one, 1, one, 1, one, two, one, 8, one, 1)
    block = (row_count, width)
    in_vmem = pl.BlockSpec(memory_space=pltpu.VMEM)
    in_any = pl.BlockSpec(memory_space=pl.ANY)
    return pl.pallas_call(
        functools.partial(fused_kernel, groups, ranks),
        out_shape=(
            jax.ShapeDtypeStruct((queries.shape[0] // ranks, width), bf16),
            jax.ShapeDtypeStruct(block, bf16),
        ),
        in_specs=[in_vmem] * 5 + [in_any] * 7,
        out_specs=(in_any, in_any),
        scratch_shapes=[
            vmem((chips, groups, 2) + block, bf16),
            vmem((chips, groups, 2) + block, bf16),
            vmem((chips, groups) + block, bf16),
            vmem((2, chips) + block, bf16),
            vmem((chips,) + block, bf16),
            vmem((4,) + block, bf16),
            vmem((ranks,) + out_weight.shape, bf16),
            vmem((ranks, WINDOW, 128), bf16),
            vmem((chips, groups, 2, groups, 1, 128), f32),
            vmem((2, WINDOW, 128), bf16),
            vmem((2, 2 * WINDOW, 128), bf16),
            vmem((2, 2 * WINDOW, 128), bf16),
            vmem((WINDOW, ranks * 128), bf16),
            vmem((groups * 2 * row_count, units), bf16),
            vmem((queries.shape[0] // ranks, width), bf16),
            vmem(queries.shape, bf16),
            vmem(key_rows.shape, bf16),
            vmem(value_rows.shape, bf16),
            vmem((width, units), bf16),
            vmem((width, units), bf16),
            vmem((units, width), bf16),
        ]
        + [dma((count,)) for count in counts],
        compiler_params=pltpu.CompilerParams(
            collective_id=0, has_side_effects=True, vmem_limit_bytes=60 * 1024 * 1024
        ),
    )(
        routes.T,
        route_weight.T,
        sink_logits[None, :],
        moe_rows,
        moe_gain[None, :],
        queries,
        key_rows,
        value_rows,
        out_weight,
        gate_weight,
        up_weight,
        down_weight,
    )


def body(
    queries,
    key_rows,
    value_rows,
    sink_logits,
    out_weight,
    moe_rows,
    moe_gain,
    routes,
    route_weight,
    gate_weight,
    up_weight,
    down_weight,
):
    groups, ranks = lax.axis_size("ep"), lax.axis_size("tp")
    fits = groups == 4 and ranks == 8 and sink_logits.shape[0] == 2
    fits = fits and queries.shape == (ranks * WINDOW, 2 * HEAD_DIM)
    fits = fits and key_rows.shape[1] == 128 and moe_rows.shape[0] in (32, 64)
    if fits:
        return fused(
            queries,
            key_rows,
            value_rows,
            sink_logits,
            out_weight,
            moe_rows,
            moe_gain,
            routes,
            route_weight,
            gate_weight,
            up_weight,
            down_weight,
        )
    mixer_out = mixer(queries, key_rows, value_rows, sink_logits, out_weight)
    moe_out = experts(moe_rows, moe_gain, routes, route_weight, gate_weight, up_weight, down_weight)
    return (mixer_out, moe_out)


def solution(mesh):
    in_specs = (
        P("ep", "tp"),
        P("ep", None),
        P("ep", None),
        P("tp"),
        P("tp", None),
        P(("ep", "tp"), None),
        P(),
        P(("ep", "tp"), None),
        P(("ep", "tp"), None),
        P("ep", None, "tp"),
        P("ep", None, "tp"),
        P("ep", "tp", None),
    )
    out_specs = (P(("ep", "tp"), None), P(("ep", "tp"), None))
    return jax.shard_map(body, mesh=mesh, in_specs=in_specs, out_specs=out_specs, check_vma=False)
```

time: 89.3 us -> 71.6 us (0.80)
  the two profiles are of different devices: /device:TPU:0 before, /device:TPU:25 now
where the time goes in v1:
time: 71.6 us; the launch traced here: 71.4 us
  Pallas kernels  67.3 us (94%)
  local copies, waits for them, and re-layouts  3.45 us (5%)
    pallas_call x1, Pallas kernels, fused(): pl.pallas_call(functools.partial(fused_kernel, groups, ranks), out_shape=...  67.3 us
    unnamed x2, local copies, waits for them, and re-layouts  3.45 us

profile of v1, /device:TPU:25, one launch (start us, length us, event | category | flops | bytes accessed | tf_op | source)
XLA Modules:
  0.0 71.4 jit_solution(9129045220084527898)
XLA Ops:
  0.6 67.3 %shard_map.131 = (bf16[128,2048]{1,0:T(8,128)(2,1)}, bf16[32,2048]{1,0:T(8,128)(2,1)}) custom-call(s32[2,32]{1,0:T(2,128)} %bitcast.5, f32[2,32]{1,0:T(2,128)} %bitcast.6, f32[1,2]{1,0:T(1,128)} %bitcast.7, bf16[32,2048]{1,0:T(8,128)(2,1)} %rows_ref.1, f32[1,2048]{1,0:T(1,128)} %bitcast.4, bf16[1024,128]{1,0:T(8,128)(2,1)} %q_hbm.1, ...), custom_call_target="tpu_custom_call" | custom-call | tf_op jit(solution)/shard_map/pallas_call | solution.py:793
  67.9 1.9 %copy.16 = bf16[128,2048]{1,0:T(8,128)(2,1)} copy(bf16[128,2048]{1,0:T(8,128)(2,1)} %get-tuple-element.4) | data formatting | bytes 1048576
  69.8 1.6 %copy.17 = bf16[32,2048]{1,0:T(8,128)(2,1)} copy(bf16[32,2048]{1,0:T(8,128)(2,1)} %get-tuple-element.5) | data formatting | bytes 262144

commit v2 on v1

--- a/solution.py
+++ b/solution.py
@@ -18,6 +18,7 @@
 
 big_negative = -1e30
 norm_eps = 1e-05
+SHARE = 2
 
 
 def passed_along(value, axis, steps):
@@ -155,8 +156,8 @@
     gate_hbm,
     up_hbm,
     down_hbm,
-    mix_hbm,
-    moe_hbm,
+    mix_ref,
+    moe_ref,
     x_buf,
     p_buf,
     r1_buf,
@@ -171,7 +172,6 @@
     vdup,
     att,
     hid,
-    mix_v,
     q_ref,
     key_ref,
     value_ref,
@@ -179,7 +179,6 @@
     up_w,
     down_w,
     load_sem,
-    out_sem,
     sem,
     z_rs,
     x1_rs,
@@ -303,31 +302,40 @@
             remote(line, line, line_sem, zl_rs.at[zz], to).start()
 
     def spread(zz):
-        pair_send(zz, e, (x1_ss, x1_rs.at[zz]), (l1_ss, l1_rs.at[zz]), (e1, t))
+        for h in range(2):
+            part = half(x_buf.at[zz, e, c], h)
+            remote(part, part, x1_ss, x1_rs.at[zz * 2 + h], (e1, t)).start()
+        line = l_buf.at[zz, e, c]
+        remote(line, line, l1_ss, l1_rs.at[zz], (e1, t)).start()
         pair_send(zz, e, (x2_ss, x2_rs.at[zz]), (l2_ss, l2_rs.at[zz]), (e2, t))
         pair_send(zz, e, (pa_ss, pa_rs.at[zz]), (lp_ss, lp_rs.at[zz]), (e, other))
 
+    def arrive_half(i, h):
+        zz = plane(i)
+        with jax.named_scope("half%d" % h):
+            received(half(x_buf.at[zz, e, c], h), z_rs.at[zz * 2 + h])
+        if h == 1:
+            received(l_buf.at[zz, e, c], zl_rs.at[zz])
+
+        @pl.when(mid)
+        def _():
+            z_send(zz, (e, t + 2 - 4 * from_above(zz)), h, zf_ss, zlf_ss)
+
     @jax.named_scope("arrive")
     def arrive(i):
-        zz = plane(i)
-        to = (e, t + 2 - 4 * from_above(zz))
         for h in range(2):
-            received(half(x_buf.at[zz, e, c], h), z_rs.at[zz * 2 + h])
-            if h == 1:
-                received(l_buf.at[zz, e, c], zl_rs.at[zz])
-
-            @pl.when(mid)
-            def _():
-                z_send(zz, to, h, zf_ss, zlf_ss)
-
-        spread(zz)
+            arrive_half(i, h)
 
     @jax.named_scope("from_first")
     def from_first(zz):
-        received(x_buf.at[zz, e1, c], x1_rs.at[zz])
+        slot = chips + zz
+        for h in range(2):
+            part = half(x_buf.at[zz, e1, c], h)
+            received(part, x1_rs.at[zz * 2 + h])
+            remote(part, part, x2_ss, x2_rs.at[slot], (e2, t)).start()
         received(l_buf.at[zz, e1, c], l1_rs.at[zz])
-        slot = chips + zz
-        pair_send(zz, e1, (x2_ss, x2_rs.at[slot]), (l2_ss, l2_rs.at[slot]), (e2, t))
+        line = l_buf.at[zz, e1, c]
+        remote(line, line, l2_ss, l2_rs.at[slot], (e2, t)).start()
         pair_send(zz, e1, (pa_ss, pa_rs.at[zz]), (lp_ss, lp_rs.at[zz]), (e, other))
 
     @jax.named_scope("from_second")
@@ -343,14 +351,18 @@
         received(x_buf.at[zz, :, oc], pa_rs.at[zz])
         received(l_buf.at[zz, :, oc], lp_rs.at[zz])
 
-    third = w_buf.shape[1] // 4
+    all_rows = w_buf.shape[1]
+    fewer = all_rows * SHARE // 8
+    more = all_rows - fewer
     side = x * (1 - c) + y * c
-    carried = pl.ds(pl.multiple_of(side * third, third), 3 * third)
-    given = pl.ds(pl.multiple_of(3 * side * third, third), third)
-    taken = pl.ds(pl.multiple_of(3 * (1 - side) * third, third), third)
     other_side = x * c + y * (1 - c)
-    other_carried = pl.ds(pl.multiple_of(other_side * third, third), 3 * third)
-    other_taken = pl.ds(pl.multiple_of(3 * (1 - other_side) * third, third), third)
+
+    def span(which, step, size):
+        return pl.ds(pl.multiple_of(which * step, 16), size)
+
+    carried, given = span(side, fewer, more), span(side, more, fewer)
+    taken = span(1 - side, more, fewer)
+    other_carried, other_taken = span(other_side, fewer, more), span(1 - other_side, more, fewer)
 
     def w_send(zz, to, send_sem):
         block = w_buf.at[zz * 2 + c, carried, :]
@@ -403,25 +415,40 @@
 
     spread(z)
     loads[0].wait()
-    ahead = (e, t + 2 - 4 * from_above(plane(1)))
+    toward = t - 2 + 4 * from_above(plane(1))
 
     @pl.when(edge)
     def _():
-        w_send(z, (e, jnp.where(z == 0, t + 2, t - 2)), wo_ss)
+        w_send(z, (e, toward), wo_ss)
 
     w_partner(z)
     w_rest(z)
-    from_first(z)
-    arrive(1)
 
     @pl.when(mid)
     def _():
-        w_send(z, ahead, wo_ss)
-        arrive(2)
+        for h in range(2):
+            arrive_half(1, h)
+            arrive_half(2, h)
+        w_send(z, (e, 2 * t - toward), wo_ss)
+
+    pl.when(edge)(functools.partial(arrive, 1))
+    from_first(z)
+    spread(plane(1))
+    pl.when(edge)(functools.partial(arrive, 2))
+    spread(plane(2))
+
+    @pl.when(mid)
+    def _():
         arrive(3)
-        w_send(z, (e, t - 2 + 4 * from_above(plane(1))), wo_ss)
+        w_send(z, (e, toward), wo_ss)
 
     from_second(z)
+
+    @pl.when(mid)
+    def _():
+        from_first(plane(1))
+        spread(plane(3))
+
     from_partner(z)
     for load in loads[1:4]:
         load.wait()
@@ -468,43 +495,60 @@
         for n, column in enumerate((e3, e2, e1, e)):
             block = p_buf.at[zz, column, c]
             add_in(block, r1_buf.at[zz, column])
-            if n < 2:
-                place = (1 - n) * chips + zz
-                remote(block, r2_buf.at[1 - n, zz], s2_ss, s2_rs.at[place], (e2, t)).start()
+            if n == 0:
+                for h in range(2):
+                    part, into = half(block, h), half(r2_buf.at[1, zz], h)
+                    remote(part, into, s2_ss, s2_rs.at[chips + zz * 2 + h], (e2, t)).start()
+            if n == 1:
+                remote(block, r2_buf.at[0, zz], s2_ss, s2_rs.at[zz], (e2, t)).start()
 
     @jax.named_scope("second")
     def second(i):
         zz = plane(i)
-        received(r2_buf.at[1, zz], s2_rs.at[chips + zz])
-        block = p_buf.at[zz, e1, c]
-        add_in(block, r2_buf.at[1, zz])
-        remote(block, r3_buf.at[zz], s3_ss, s3_rs.at[zz], (e1, t)).start()
+        for h in range(2):
+            extra, part = half(r2_buf.at[1, zz], h), half(p_buf.at[zz, e1, c], h)
+            received(extra, s2_rs.at[chips + zz * 2 + h])
+            add_in(part, extra)
+            into = half(r3_buf.at[zz], h)
+            remote(part, into, s3_ss, s3_rs.at[zz * 2 + h], (e1, t)).start()
 
     @jax.named_scope("third_sum")
-    def third_sum(i):
+    def third_half(i, h):
         zz = plane(i)
-        received(r2_buf.at[0, zz], s2_rs.at[zz])
-        received(r3_buf.at[zz], s3_rs.at[zz])
-        block = p_buf.at[zz, e, c]
-        block[...] = (
-            block[...].astype(jnp.float32)
-            + r2_buf[0, zz].astype(jnp.float32)
-            + r3_buf[zz].astype(jnp.float32)
+        if h == 0:
+            received(r2_buf.at[0, zz], s2_rs.at[zz])
+        received(half(r3_buf.at[zz], h), s3_rs.at[zz * 2 + h])
+        part = half(p_buf.at[zz, e, c], h)
+        part[...] = (
+            part[...].astype(jnp.float32)
+            + half(r2_buf.at[0, zz], h)[...].astype(jnp.float32)
+            + half(r3_buf.at[zz], h)[...].astype(jnp.float32)
         ).astype(jnp.bfloat16)
 
-    @jax.named_scope("chain")
-    def chain(i, passing):
+    def chain_half(i, h, passing):
         zz = plane(i)
         hops = 2 if passing and i == 3 else 1
         to = (e, t + hops * (4 * from_above(zz) - 2))
         slot = 2 if i == 1 else 3 if passing else i - 2
+        part = half(p_buf.at[zz, e, c], h)
+        if passing:
+            extra = half(rc_buf.at[i - 2], h)
+            received(extra, rc_rs.at[(i - 2) * 2 + h])
+            add_in(part, extra)
+        remote(part, half(rc_buf.at[slot], h), rc_ss, rc_rs.at[slot * 2 + h], to).start()
+
+    def third_sum(i):
         for h in range(2):
-            part = half(p_buf.at[zz, e, c], h)
-            if passing:
-                extra = half(rc_buf.at[i - 2], h)
-                received(extra, rc_rs.at[(i - 2) * 2 + h])
-                add_in(part, extra)
-            remote(part, half(rc_buf.at[slot], h), rc_ss, rc_rs.at[slot * 2 + h], to).start()
+            third_half(i, h)
+            if i == 1:
+                chain_half(i, h, False)
+            if i > 1:
+                pl.when(edge)(functools.partial(chain_half, i, h, False))
+
+    @jax.named_scope("chain")
+    def chain(i):
+        for h in range(2):
+            chain_half(i, h, True)
 
     @pl.loop(0, groups)
     def _(i):
@@ -512,43 +556,43 @@
 
         @pl.when(i > 0)
         def _():
-            from_second(zz)
             from_partner(zz)
             q_send(zz)
 
         gate_up(zz, 0, cut)
 
+        @pl.when((i == 0) & edge)
+        def _():
+            from_first(plane(1))
+
+        @pl.when((i == 1) & mid)
+        def _():
+            from_first(plane(3))
+            w_arrive(2)
+
+        @pl.when(i == 2)
+        def _():
+            fold(1)
+
+        @pl.when(i == 3)
+        def _():
+            fold(2)
+
+        gate_up(zz, cut, units)
+
         @pl.when(i == 0)
         def _():
-            from_first(plane(1))
-            pl.when(edge)(functools.partial(arrive, 2))
-
-        @pl.when(i == 1)
-        def _():
-            from_first(plane(2))
+            loads[6].wait()
+
+        @pl.when((i == 1) & mid)
+        def _():
+            fold(0)
+            from_second(plane(2))
 
         @pl.when(i == 2)
         def _():
-            fold(0)
-
-        @pl.when(i == 3)
-        def _():
-            fold(2)
-            second(0)
-
-        gate_up(zz, cut, units)
-
-        @pl.when(i == 0)
-        def _():
-            loads[6].wait()
-
-        @pl.when(i == 1)
-        def _():
-            from_first(plane(3))
-
-        @pl.when(i == 2)
-        def _():
-            fold(1)
+            from_second(plane(3))
+            pl.when(mid)(functools.partial(w_arrive, 3))
 
         @pl.when(i == 3)
         def _():
@@ -571,31 +615,27 @@
             p_buf[zz] = (down * share).astype(jnp.bfloat16).reshape(groups, 2, row_count, width)
         remote(p_buf.at[zz, :, oc], r1_buf.at[zz], s1_ss, s1_rs.at[zz], (e, other)).start()
 
-        @pl.when((i == 0) & edge)
-        def _():
-            arrive(3)
-
-        @pl.when((i == 1) & mid)
-        def _():
-            w_arrive(1)
-
-        @pl.when((i == 2) & mid)
-        def _():
-            w_arrive(2)
-
-    third_sum(0)
-    third_sum(1)
-    chain(1, False)
-    second(2)
-    fold(3)
-
-    @pl.when(edge)
-    def _():
-        w_arrive(1)
-
-    @pl.when(mid)
-    def _():
-        w_arrive(3)
+        @pl.when(i == 0)
+        def _():
+            from_first(plane(2))
+            pl.when(mid)(functools.partial(w_arrive, 1))
+            from_second(plane(1))
+
+            @pl.when(edge)
+            def _():
+                arrive(3)
+                spread(plane(3))
+
+        @pl.when((i == 1) & edge)
+        def _():
+            from_second(plane(2))
+            from_first(plane(3))
+            fold(0)
+
+        @pl.when(i == 2)
+        def _():
+            second(0)
+            pl.when(edge)(functools.partial(w_arrive, 1))
 
     qb_buf[t] = q_ref[pl.ds(pl.multiple_of(t * WINDOW, WINDOW), WINDOW), :]
 
@@ -632,18 +672,18 @@
     first = jnp.where(me == 0, WINDOW, 0)
     allowed = (key_pos <= query_pos) & (key_pos > query_pos - WINDOW) & (key_pos >= first)
 
+    def q_wait(i):
+        if i == 0:
+            received(qb_buf.at[0], q_rs.at[z])
+        else:
+            received(qb_buf.at[0:2], q_rs.at[plane(i)])
+
     @jax.named_scope("attend")
-    def attend_plane(i):
-        zz = plane(i)
-        if i == 0:
-            received(qb_buf.at[0], q_rs.at[zz])
-        else:
-            received(qb_buf.at[0:2], q_rs.at[zz])
-
-        @pl.loop(0, 2)
-        def _(core):
+    def attend(begin, end):
+        for n in range(begin, end):
+            zz, core = plane(n // 2), n % 2
             j = zz * 2 + core
-            pair = qb_buf[j]
+            pair = qb_buf[j] * jnp.asarray(HEAD_DIM ** (-0.5), jnp.bfloat16)
             kept = lax.div(j * KV_HEADS, ranks)
             keys, vals = kdup[kept], vdup[kept]
             line = l_buf[zz, e, core, e]
@@ -653,50 +693,38 @@
                 query = jnp.where(mine_half, pair, jnp.zeros_like(pair))
                 scores = lax.dot_general(
                     query, keys, (((1,), (1,)), ((), ())), preferred_element_type=jnp.float32
-                ) * HEAD_DIM ** (-0.5)
+                )
                 masked = jnp.where(allowed, scores, big_negative)
                 sink = line[:, row_count + i : row_count + i + 1]
                 row_max = jnp.maximum(jnp.max(masked, -1, keepdims=True), sink)
                 powers = jnp.exp(masked - row_max)
                 totals = jnp.sum(powers, -1, keepdims=True) + jnp.exp(sink - row_max)
-                probs = (powers / totals).astype(jnp.bfloat16)
+                probs = (powers * (1.0 / totals)).astype(jnp.bfloat16)
                 outs.append(jnp.dot(probs, vals, preferred_element_type=jnp.float32))
             att[:, pl.ds(pl.multiple_of(j * 128, 128), 128)] = jnp.where(low, outs[0], outs[1]).astype(
                 jnp.bfloat16
             )
 
-    attend_plane(0)
+    q_wait(0)
+    attend(0, 1)
+    fold(3)
+    second(2)
+    pl.when(edge)(functools.partial(w_arrive, 2))
+    attend(1, 2)
+    q_wait(1)
+    attend(2, 4)
+    third_sum(1)
+    second(3)
     third_sum(2)
-
-    @pl.when(edge)
-    def _():
-        chain(2, False)
-
-    second(3)
-    attend_plane(1)
-
-    @pl.when(mid)
-    def _():
-        chain(2, True)
-
+    pl.when(edge)(functools.partial(w_arrive, 3))
+    q_wait(2)
+    attend(4, 6)
     third_sum(3)
-
-    @pl.when(edge)
-    def _():
-        chain(3, False)
-        w_arrive(2)
-
-    attend_plane(2)
-
-    @pl.when(mid)
-    def _():
-        chain(3, True)
-
-    attend_plane(3)
-
-    @pl.when(edge)
-    def _():
-        w_arrive(3)
+    pl.when(mid)(functools.partial(chain, 2))
+    q_wait(3)
+    attend(6, ranks)
+    pl.when(mid)(functools.partial(chain, 3))
+    third_sum(0)
 
     with jax.named_scope("wwait"):
         for i in range(1, chips):
@@ -706,21 +734,17 @@
         received(w_buf.at[0:chips, other_carried, :], wp_rs.at[0])
         received(w_buf.at[0:chips, other_taken, :], wq_rs.at[0])
     with jax.named_scope("mix"):
-        mix_v[...] = jnp.dot(
+        mix_ref[...] = jnp.dot(
             att[...], w_buf[...].reshape(ranks * 128, width), preferred_element_type=jnp.float32
         ).astype(jnp.bfloat16)
-    mix_out = pltpu.make_async_copy(mix_v, mix_hbm, out_sem.at[0])
-    mix_out.start()
-
-    for slot in (2, 3):
-        for h in range(2):
-            part = half(rc_buf.at[slot], h)
-            with jax.named_scope("last"):
+    for h in range(2):
+        with jax.named_scope("last"):
+            total = half(p_buf.at[z, e, c], h)[...].astype(jnp.float32)
+            for slot in (2, 3):
+                part = half(rc_buf.at[slot], h)
                 received(part, rc_rs.at[slot * 2 + h])
-                add_in(half(p_buf.at[z, e, c], h), part)
-
-    moe_out = pltpu.make_async_copy(p_buf.at[z, e, c], moe_hbm, out_sem.at[1])
-    moe_out.start()
+                total = total + part[...].astype(jnp.float32)
+            half(moe_ref, h)[...] = total.astype(jnp.bfloat16)
 
     sent(r1_buf.at[0], x1_ss)
     sent(r1_buf.at[0:2], x2_ss)
@@ -728,7 +752,7 @@
     sent(l_buf.at[0, :, 0], l1_ss)
     sent(l_buf.at[0], l2_ss)
     sent(l_buf.at[0:2], lp_ss)
-    heavy, light = pl.ds(0, 3 * third), pl.ds(0, third)
+    heavy, light = pl.ds(0, more), pl.ds(0, fewer)
 
     @pl.when(edge)
     def _():
@@ -745,6 +769,7 @@
         sent(l_buf.at[0, 0:3, 0], zlf_ss)
         sent(w_buf.at[0:3, heavy, :], wf_ss)
 
+
     sent(w_buf.at[0:chips, heavy, :], wp_ss)
     sent(w_buf.at[0:chips, light, :], wq_ss)
     sent(w_buf.at[0 : chips - 1, light, :], wx_ss)
@@ -757,10 +782,6 @@
     @pl.when(gives)
     def _():
         sent(halo, halo_ss)
-
-    with jax.named_scope("outs"):
-        mix_out.wait()
-        moe_out.wait()
 
 
 def fused(
@@ -785,19 +806,19 @@
     vmem = pltpu.VMEM
     dma = pltpu.SemaphoreType.DMA
     one, two = chips, 2 * chips
-    counts = (7, 2, 21, two, one, two, one, one, one, two, one)
-    counts += (one, 1, one, 1, one, two, one, 8, one, 1)
+    counts = (7, 21, two, two, two, one, one, one, two, one)
+    counts += (one, 1, one, 1, one, 3 * chips, two, 8, one, 1)
     block = (row_count, width)
     in_vmem = pl.BlockSpec(memory_space=pltpu.VMEM)
     in_any = pl.BlockSpec(memory_space=pl.ANY)
     return pl.pallas_call(
         functools.partial(fused_kernel, groups, ranks),
         out_shape=(
-            jax.ShapeDtypeStruct((queries.shape[0] // ranks, width), bf16),
-            jax.ShapeDtypeStruct(block, bf16),
+            pltpu.VMEM((queries.shape[0] // ranks, width), bf16),
+            pltpu.VMEM(block, bf16),
         ),
         in_specs=[in_vmem] * 5 + [in_any] * 7,
-        out_specs=(in_any, in_any),
+        out_specs=(in_vmem, in_vmem),
         scratch_shapes=[
             vmem((chips, groups, 2) + block, bf16),
             vmem((chips, groups, 2) + block, bf16),
@@ -813,7 +834,6 @@
             vmem((2, 2 * WINDOW, 128), bf16),
             vmem((WINDOW, ranks * 128), bf16),
             vmem((groups * 2 * row_count, units), bf16),
-            vmem((queries.shape[0] // ranks, width), bf16),
             vmem(queries.shape, bf16),
             vmem(key_rows.shape, bf16),
             vmem(value_rows.shape, bf16),

time: 71.6 us -> 61.7 us (0.86)
  the two profiles are of different devices: /device:TPU:25 before, /device:TPU:0 now
where the time goes in v2:
time: 61.7 us; the launch traced here: 61.5 us
  Pallas kernels  59.4 us (96%)
  local copies, waits for them, and re-layouts  1.45 us (2%)
  between operations  0.64 us (1%)
    pallas_call x1, Pallas kernels, fused(): pl.pallas_call(functools.partial(fused_kernel, groups, ranks), out_shape=...  59.4 us
    unnamed x2, local copies, waits for them, and re-layouts  1.45 us

profile of v2, /device:TPU:0, one launch (start us, length us, event | category | flops | bytes accessed | tf_op | source)
XLA Modules:
  0.0 61.5 jit_solution(14377085703967681885)
XLA Ops:
  0.6 59.4 %shard_map.131 = (bf16[128,2048]{1,0:T(8,128)(2,1)S(1)}, bf16[32,2048]{1,0:T(8,128)(2,1)S(1)}) custom-call(s32[2,32]{1,0:T(2,128)} %bitcast.5, f32[2,32]{1,0:T(2,128)} %bitcast.6, f32[1,2]{1,0:T(1,128)} %bitcast.7, bf16[32,2048]{1,0:T(8,128)(2,1)} %rows_ref.1, f32[1,2048]{1,0:T(1,128)} %bitcast.4, bf16[1024,128]{1,0:T(8,128)(2,1)} %q_hbm.1, ...), custom_call_target="tpu_custom_call" | custom-call | tf_op jit(solution)/shard_map/pallas_call | solution.py:814
  60.1 0.8 %copy.16 = bf16[128,2048]{1,0:T(8,128)(2,1)} copy(bf16[128,2048]{1,0:T(8,128)(2,1)S(1)} %get-tuple-element.2) | data formatting | bytes 1048576
  60.9 0.7 %copy.17 = bf16[32,2048]{1,0:T(8,128)(2,1)} copy(bf16[32,2048]{1,0:T(8,128)(2,1)S(1)} %get-tuple-element.3) | data formatting | bytes 262144
